TPU v7x, 32 devices: a whole 2x2x4 slice. The times are simulated.
32 devices in a mesh: fs: 4 (over z), rep: 4 (over y, x), tp: 2 (over core).
Axes of the slice: x: 2, y: 2, z: 4, core: 2. Of those that a mesh axis runs over, the one named last changes fastest.
Arguments:
- saved_latent: bfloat16 [12288, 2048], P(('fs', 'rep')), may hold values from -6 to 6
- query_cotangent: bfloat16 [12288, 3072], P(('fs', 'rep'), 'tp'), may hold values from -6 to 6
- mix_cotangent: bfloat16 [12288, 4096], P(('fs', 'rep')), may hold values from -6 to 6
- head_outputs: bfloat16 [12288, 2048], P(('fs', 'rep'), 'tp'), may hold values from -6 to 6
- query_weight: float32 [2048, 3072], P('fs', 'tp'), may hold values from -0.125 to 0.125
- out_weight: float32 [4096, 2048], P('fs', 'tp'), may hold values from -0.125 to 0.125
- query_basis: bfloat16 [2048, 256], replicated, may hold values from -0.125 to 0.125
- out_basis: bfloat16 [4096, 256], replicated, may hold values from -0.09375 to 0.09375
- query_mean: float32 [256, 3072], P('fs', 'tp'), may hold values from -3 to 3
- query_var: float32 [256, 3072], P('fs', 'tp'), may hold values from 0.1 to 1
- out_mean: float32 [256, 2048], P('fs', 'tp'), may hold values from -3 to 3
- out_var: float32 [256, 2048], P('fs', 'tp'), may hold values from 0.1 to 1
Outputs:
- query_step: float32 [2048, 3072], P('fs', 'tp')
- out_step: float32 [4096, 2048], P('fs', 'tp')
- query_copy: bfloat16 [2048, 3072], P('fs', 'tp')
- out_copy: bfloat16 [4096, 2048], P('fs', 'tp')
All inputs are finite; a program needn't handle non-finite values.
Results may differ from a plain program's by a relative error of at most 0.001.
Values sent between devices are 32-bit elements; how exact they have to be, the bound alone decides.
A program may use at most 128 MiB of HBM per device.

v0:
```python
import jax
import jax.numpy as jnp
from jax import lax
from jax.sharding import PartitionSpec as P


def token_sum(left, right):
    return lax.dot_general(
        left, right, (((0,), (0,)), ((), ())), preferred_element_type=jnp.float32
    )


def project(basis, grad):
    return lax.dot_general(
        basis.astype(jnp.float32), grad, (((0,), (0,)), ((), ())), precision=lax.Precision.HIGHEST
    )


def moment_direction(proj, scale, mean, var):
    scaled = scale * proj
    new_mean = 0.8 * mean + 0.2 * scaled
    new_var = 0.9 * var + 0.1 * scaled * scaled
    return new_mean / jnp.sqrt(new_var)


def on_device(
    saved_latent,
    query_cotangent,
    mix_cotangent,
    head_outputs,
    query_weight,
    out_weight,
    query_basis,
    out_basis,
    query_mean,
    query_var,
    out_mean,
    out_var,
):
    query_rows = query_weight.shape[0]
    out_rows = out_weight.shape[0]
    position = lax.axis_index("fs")
    query_local = lax.dynamic_slice_in_dim(query_basis, position * query_rows, query_rows, 0)
    out_local = lax.dynamic_slice_in_dim(out_basis, position * out_rows, out_rows, 0)
    query_early = project(query_basis, token_sum(saved_latent, query_cotangent))
    out_early = project(out_basis, token_sum(mix_cotangent, head_outputs))
    query_shard, out_shard = (
        lax.psum_scatter(query_early, "fs", scatter_dimension=0, tiled=True),
        lax.psum_scatter(out_early, "fs", scatter_dimension=0, tiled=True),
    )
    query_proj, out_proj = lax.psum((query_shard, out_shard), "rep")
    query_squares, out_squares = lax.psum(
        (jnp.sum(query_proj * query_proj), jnp.sum(out_proj * out_proj)), ("fs", "tp")
    )
    spread = lax.axis_size("fs") * lax.axis_size("tp")
    query_count = float(query_proj.shape[0] * query_proj.shape[1] * spread)
    out_count = float(out_proj.shape[0] * out_proj.shape[1] * spread)
    query_scale = 1.0 / jnp.maximum(jnp.sqrt(query_squares / query_count), 1.0)
    out_scale = 1.0 / jnp.maximum(jnp.sqrt(out_squares / out_count), 1.0)
    query_dir = moment_direction(query_proj, query_scale, query_mean, query_var)
    out_dir = moment_direction(out_proj, out_scale, out_mean, out_var)
    query_left = query_local.astype(jnp.float32)
    out_left = out_local.astype(jnp.float32)
    query_step = jnp.dot(
        query_left,
        lax.all_gather(query_dir, "fs", axis=0, tiled=True),
        precision=lax.Precision.HIGHEST,
    )
    out_step = jnp.dot(
        out_left, lax.all_gather(out_dir, "fs", axis=0, tiled=True), precision=lax.Precision.HIGHEST
    )
    query_copy = (query_weight - 0.05 * query_step).astype(jnp.bfloat16)
    out_copy = (out_weight - 0.05 * out_step).astype(jnp.bfloat16)
    return (query_step, out_step, query_copy, out_copy)


def solution(mesh):
    placed = (
        P(("fs", "rep"), None),
        P(("fs", "rep"), "tp"),
        P(("fs", "rep"), None),
        P(("fs", "rep"), "tp"),
        P("fs", "tp"),
        P("fs", "tp"),
        P(),
        P(),
        P("fs", "tp"),
        P("fs", "tp"),
        P("fs", "tp"),
        P("fs", "tp"),
    )
    return jax.shard_map(
        on_device,
        mesh=mesh,
        in_specs=placed,
        out_specs=(P("fs", "tp"), P("fs", "tp"), P("fs", "tp"), P("fs", "tp")),
        check_vma=False,
    )
```

profile of v0, /device:TPU:0, one launch (start us, length us, event | category | flops | bytes accessed | tf_op | source)
XLA Modules:
  0.0 249.4 jit_solution(1730076010502316369)
XLA Ops:
  7.2 0.0 copy-start
  7.2 0.0 reduce-scatter.9.cloned.1.call-start
  7.2 0.0 copy-start.2
  7.2 9.7 %fusion.13 = f32[4096,1024]{1,0:T(8,128)S(1)} fusion(bf16[768,4096]{1,0:T(8,128)(2,1)} %param.14, bf16[768,1024]{1,0:T(8,128)(2,1)} %param.15), kind=kOutput, calls=%fused_computation.21 | convolution fusion | flops 6442450944 | bytes 24641536 | tf_op jit(solution)/shard_map/dot_general | solution.py:8
  16.9 0.0 copy-done.2
  16.9 14.3 %convolution_bitcast_fusion.1 = f32[256,1024]{0,1:T(8,128)} fusion(f32[4096,1024]{1,0:T(8,128)S(1)} %fusion.13, bf16[4096,256]{1,0:T(8,128)(2,1)S(1)} %copy-done.2), kind=kOutput, calls=%fused_computation.3 | convolution fusion | flops 12884901888 | bytes 19922944 | tf_op jit(solution)/shard_map/dot_general | solution.py:14
  31.2 2.5 %copy.30 = f32[256,1024]{1,0:T(8,128)} copy(f32[256,1024]{0,1:T(8,128)} %convolution_bitcast_fusion.1) | data formatting | bytes 2097152
  33.8 0.0 reduce-scatter.9.cloned.1.call-update
  33.8 0.0 reduce-scatter.7.cloned.1.call-start
  33.8 0.0 copy-done
  33.9 0.0 copy-start.3
  33.9 7.0 %fusion.12 = f32[2048,1536]{1,0:T(8,128)S(1)} fusion(bf16[768,2048]{1,0:T(8,128)(2,1)S(1)} %copy-done, bf16[768,1536]{1,0:T(8,128)(2,1)} %param.13), kind=kOutput, calls=%fused_computation.20 | convolution fusion | flops 4831838208 | bytes 18087936 | tf_op jit(solution)/shard_map/dot_general | solution.py:8
  40.9 0.0 copy-done.3
  40.9 10.6 %convolution_bitcast_fusion = f32[256,1536]{0,1:T(8,128)S(1)} fusion(f32[2048,1536]{1,0:T(8,128)S(1)} %fusion.12, bf16[2048,256]{1,0:T(8,128)(2,1)S(1)} %copy-done.3), kind=kOutput, calls=%fused_computation.2 | convolution fusion | flops 9663676416 | bytes 15204352 | tf_op jit(solution)/shard_map/dot_general | solution.py:14
  51.6 0.0 copy-start.6
  51.6 0.0 copy-start.7
  51.6 0.0 copy-start.4
  51.6 0.0 copy-start.5
  51.6 1.6 copy.28
  53.2 0.0 reduce-scatter.7.cloned.1.call-update
  53.3 0.0 all-reduce.4.cloned.1.call-start
  53.3 10.6 %reduce-scatter.9.cloned.1.call-done = f32[64,1024]{1,0:T(8,128)} async-done(((f32[256,1024]{1,0:T(8,128)}), f32[64,1024]{1,0:T(8,128)}) %reduce-scatter.9.cloned.1.call-update) | async-done | bytes 262160 | tf_op jit(solution)/shard_map/reduce_scatter | solution.py:49
  64.0 36.9 %reduce-scatter.7.cloned.1.call-done = f32[64,1536]{1,0:T(8,128)} async-done(((f32[256,1536]{1,0:T(8,128)}), f32[64,1536]{1,0:T(8,128)}) %reduce-scatter.7.cloned.1.call-update) | async-done | bytes 393232 | tf_op jit(solution)/shard_map/reduce_scatter | solution.py:48
  100.8 0.0 all-reduce.4.cloned.1.call-update
  100.8 0.0 all-gather.5.cloned.1.call-start
  100.9 48.7 %all-reduce.4.cloned.1.call-done = (f32[64,1536]{1,0:T(8,128)}, f32[64,1024]{1,0:T(8,128)}) async-done(((f32[64,1536]{1,0:T(8,128)}, f32[64,1024]{1,0:T(8,128)}), (f32[64,1536]{1,0:T(8,128)}, f32[64,1024]{1,0:T(8,128)})) %all-reduce.4.cloned.1.call-update) | async-done | bytes 655376 | tf_op jit(solution)/shard_map/psum | solution.py:51
  149.6 1.7 multiply_reduce_fusion
  151.3 1.6 multiply_reduce_fusion.1
  152.9 16.9 %all-reduce = (f32[]{:T(128)}, f32[]{:T(128)}) all-reduce(f32[]{:T(128)} %multiply_reduce_fusion, f32[]{:T(128)} %multiply_reduce_fusion.1), channel_id=1, replica_groups=mesh['fs'=4,'rep'=4,'tp'=2] {'fs','tp'}, use_global_device_ids=true, to_apply=%region_3.0 | all-reduce | flops 2 | bytes 16 | tf_op jit(solution)/shard_map/psum | solution.py:52
  170.5 0.0 copy-done.6
  170.5 0.0 copy-done.7
  170.6 1.7 fusion.7
  172.3 0.0 all-gather.5.cloned.1.call-update
  172.3 0.0 all-gather.3.cloned.1.call-start
  173.1 0.0 copy-done.4
  173.1 0.0 copy-done.5
  173.1 1.9 fusion.4
  175.0 0.0 all-gather.3.cloned.1.call-update
  175.0 22.7 %all-gather.5.cloned.1.call-done = f32[256,1024]{1,0:T(8,128)} async-done(((f32[64,1024]{1,0:T(8,128)}), f32[256,1024]{1,0:T(8,128)}) %all-gather.5.cloned.1.call-update) | async-done | bytes 1048592 | tf_op jit(solution)/shard_map/all_gather | solution.py:70
  197.7 0.0 copy-start.1
  197.7 7.6 %subtract_convert_fusion = (bf16[1024,1024]{1,0:T(8,128)(2,1)}, f32[1024,1024]{1,0:T(8,128)}) fusion(f32[1024,1024]{1,0:T(8,128)} %param.17, f32[256,1024]{1,0:T(8,128)} %all-gather.5.cloned.1.call-done, bf16[4096,256]{1,0:T(8,128)(2,1)} %param.19, s32[]{:T(128)S(6)} %select_n.7), kind=kOutput, calls=%fused_computation | convolution fusion | flops 3224371200 | bytes 12058628 | tf_op jit(solution)/shard_map/dot_general | solution.py:69
  205.3 30.8 %all-gather.3.cloned.1.call-done = f32[256,1536]{1,0:T(8,128)} async-done(((f32[64,1536]{1,0:T(8,128)}), f32[256,1536]{1,0:T(8,128)}) %all-gather.3.cloned.1.call-update) | async-done | bytes 1572880 | tf_op jit(solution)/shard_map/all_gather | solution.py:66
  236.1 6.3 %subtract_convert_fusion.1 = (bf16[512,1536]{1,0:T(8,128)(2,1)}, f32[512,1536]{1,0:T(8,128)}) fusion(f32[512,1536]{1,0:T(8,128)} %param.16, f32[256,1536]{1,0:T(8,128)} %all-gather.3.cloned.1.call-done, bf16[2048,256]{1,0:T(8,128)(2,1)} %param.18, s32[]{:T(128)S(6)} %select_n.6), kind=kOutput, calls=%fused_computation.1 | convolution fusion | flops 2418278400 | bytes 9699332 | tf_op jit(solution)/shard_map/dot_general | solution.py:64
  242.4 0.0 copy-done.1
Async XLA Ops:
  7.2 26.7 %copy-start = (bf16[768,2048]{1,0:T(8,128)(2,1)S(1)}, bf16[768,2048]{1,0:T(8,128)(2,1)}, u32[]{:S(2)}) copy-start(bf16[768,2048]{1,0:T(8,128)(2,1)} %param.12) | copy-start | bytes 9437188
  7.2 56.8 %reduce-scatter.9.cloned.1.call-start = ((), (), s32[]{:S(2)}) async-start(), calls=%async_computation.5 | async-start | bytes 1310720 | tf_op jit(solution)/shard_map/reduce_scatter | solution.py:49
  7.2 9.7 %copy-start.2 = (bf16[4096,256]{1,0:T(8,128)(2,1)S(1)}, bf16[4096,256]{1,0:T(8,128)(2,1)}, u32[]{:S(2)}) copy-start(bf16[4096,256]{1,0:T(8,128)(2,1)} %param.19) | copy-start | bytes 6291460
  33.8 67.0 %reduce-scatter.7.cloned.1.call-start = ((), (), s32[]{:S(2)}) async-start(), calls=%async_computation.4 | async-start | bytes 1966080 | tf_op jit(solution)/shard_map/reduce_scatter | solution.py:48
  33.9 7.1 %copy-start.3 = (bf16[2048,256]{1,0:T(8,128)(2,1)S(1)}, bf16[2048,256]{1,0:T(8,128)(2,1)}, u32[]{:S(2)}) copy-start(bf16[2048,256]{1,0:T(8,128)(2,1)} %param.18) | copy-start | bytes 3145732
  51.6 119.0 %copy-start.6 = (f32[64,1024]{1,0:T(8,128)S(1)}, f32[64,1024]{1,0:T(8,128)}, u32[]{:S(2)}) copy-start(f32[64,1024]{1,0:T(8,128)} %param.23) | copy-start | bytes 786436
  51.6 119.0 %copy-start.7 = (f32[64,1024]{1,0:T(8,128)S(1)}, f32[64,1024]{1,0:T(8,128)}, u32[]{:S(2)}) copy-start(f32[64,1024]{1,0:T(8,128)} %param.22) | copy-start | bytes 786436
  51.6 121.5 %copy-start.4 = (f32[64,1536]{1,0:T(8,128)S(1)}, f32[64,1536]{1,0:T(8,128)}, u32[]{:S(2)}) copy-start(f32[64,1536]{1,0:T(8,128)} %param.21) | copy-start | bytes 1179652
  51.6 121.5 %copy-start.5 = (f32[64,1536]{1,0:T(8,128)S(1)}, f32[64,1536]{1,0:T(8,128)}, u32[]{:S(2)}) copy-start(f32[64,1536]{1,0:T(8,128)} %param.20) | copy-start | bytes 1179652
  53.3 96.3 %all-reduce.4.cloned.1.call-start = ((), (), s32[]{:S(2)}) async-start(), calls=%async_computation.6 | async-start | bytes 1310720 | tf_op jit(solution)/shard_map/psum | solution.py:51
  100.8 96.9 %all-gather.5.cloned.1.call-start = ((), (), s32[]{:S(2)}) async-start(), calls=%async_computation.3 | async-start | bytes 1310720 | tf_op jit(solution)/shard_map/all_gather | solution.py:70
  172.3 63.8 %all-gather.3.cloned.1.call-start = ((), (), s32[]{:S(2)}) async-start(), calls=%async_computation.2 | async-start | bytes 1966080 | tf_op jit(solution)/shard_map/all_gather | solution.py:66
  197.7 44.7 %copy-start.1 = (bf16[768,2048]{1,0:T(8,128)(2,1)S(1)}, bf16[768,2048]{1,0:T(8,128)(2,1)}, u32[]{:S(2)}) copy-start(bf16[768,2048]{1,0:T(8,128)(2,1)} %param.12) | copy-start | bytes 9437188
Sparse Core Ops, SparseCore 0:
  33.9 29.9 reduce-scatter.8
  66.8 33.9 reduce-scatter.6
  103.9 45.6 all-reduce.3
  172.4 25.2 all-gather.4
  199.7 36.3 all-gather.2
where the time goes:
time: 253 us; the launch traced here: 249 us
  waiting for transfers between devices  150 us (59%)
  matrix products  55.5 us (22%)
  blocking collectives  16.9 us (7%)
  between operations  15.8 us (6%)
  other arithmetic  6.95 us (3%)
  local copies, waits for them, and re-layouts  4.2 us (2%)
    psum x1, waiting for transfers between devices, on_device(): query_proj, out_proj = lax.psum((query_shard, out_shard), 'rep')  48.7 us
    reduce_scatter x1, waiting for transfers between devices, on_device(): lax.psum_scatter(query_early, 'fs', scatter_dimension=0, tiled=True)  36.9 us
    all_gather x1, waiting for transfers between devices, on_device(): lax.all_gather(query_dir, 'fs', axis=0, tiled=True)  30.8 us
    dot_general x2, matrix products, project(): lax.dot_general(basis.astype(jnp.float32), grad, (((0,), (0,)), ((), ()))...  24.9 us
    all_gather x1, waiting for transfers between devices, on_device(): lax.all_gather(out_dir, 'fs', axis=0, tiled=True)  22.7 us
    psum x1, blocking collectives, on_device(): lax.psum((jnp.sum(query_proj * query_proj), jnp.sum(out_proj * out_proj))...  16.9 us
    dot_general x2, matrix products, token_sum(): lax.dot_general(left, right, (((0,), (0,)), ((), ())), preferred_element_...  16.7 us
    reduce_scatter x1, waiting for transfers between devices, on_device(): lax.psum_scatter(out_early, 'fs', scatter_dimension=0, tiled=True)  10.6 us
  transfers between devices with their start and end apart: 5, of which 5 were waited for; matrix products, arithmetic and copies ran while one was open for 12% of the time, Pallas kernels for 0%

commit v1 on v0

v1 whole, which is shorter than its diff:
```python
import functools

import jax
import jax.numpy as jnp
from jax import lax
from jax.experimental import pallas as pl
from jax.experimental.pallas import tpu as pltpu
from jax.sharding import PartitionSpec as P

MESH = pl.DeviceIdType.MESH
REP = 4


def flip(r, bits):
    if bits == 1:
        return r + 1 - 2 * lax.rem(r, 2)
    if bits == 2:
        return lax.rem(r + 2, REP)
    return REP - 1 - r


class Stream:
    def __init__(self, names, refs):
        self.__dict__.update(zip(names, refs))


STREAM_IN = ("left_hbm", "right_hbm", "basis_hbm", "mean_hbm", "var_hbm")
STREAM_SCRATCH = (
    "left", "right", "basis", "mean", "var", "pair", "part", "fwd_in", "keep_in", "last_in",
    "row_in", "near", "far",
)


def exchange_kernel(n_f, n_t, n_sem, *refs):
    ins, outs, scratch = refs[:10], refs[10:12], refs[12:]
    streams = []
    per = len(STREAM_SCRATCH)
    for i in range(2):
        s = Stream(STREAM_IN, ins[5 * i : 5 * i + 5])
        s.__dict__.update(zip(STREAM_SCRATCH, scratch[per * i : per * i + per]))
        s.gathered = outs[i]
        s.width = s.part.shape[-1]
        streams.append(s)
    load_sem, send_sem, recv_sem = scratch[2 * per :]
    f, r, t = lax.axis_index("fs"), lax.axis_index("rep"), lax.axis_index("tp")
    rank = streams[0].gathered.shape[1]
    rows = rank // n_f
    half = rows // 2
    counter = [0]
    pending = []

    def send(src, dst, where):
        k = counter[0]
        counter[0] += 1
        copy = pltpu.make_async_remote_copy(
            src_ref=src, dst_ref=dst, send_sem=send_sem.at[k], recv_sem=recv_sem.at[k],
            device_id=where, device_id_type=MESH,
        )
        copy.start()
        pending.append(copy)
        return copy

    loads = {}
    slot = 0
    for i, s in enumerate(streams):
        cols = pl.ds(pl.multiple_of(r * s.width, 128), s.width)
        for name in ("basis", "left", "right", "mean", "var"):
            src = getattr(s, name + "_hbm")
            if name in ("mean", "var"):
                src = src.at[:, cols]
            copy = pltpu.make_async_copy(src, getattr(s, name), load_sem.at[slot])
            copy.start()
            loads[i, name] = copy
            slot += 1

    group = n_t * REP
    place = r * n_t + t

    def neighbour(k):
        other = lax.rem(place + k, group)
        return {"rep": other // n_t, "tp": lax.rem(other, n_t)}

    barrier = pltpu.get_barrier_semaphore()
    for k in range(1, group):
        pl.semaphore_signal(barrier, inc=1, device_id=neighbour(k), device_id_type=MESH)
    for k in range(1, n_f):
        pl.semaphore_signal(
            barrier, inc=1, device_id={"fs": lax.rem(f + k, n_f)}, device_id_type=MESH
        )

    def token_product(i, s):
        loads[i, "basis"].wait()
        loads[i, "left"].wait()
        tokens = s.left.shape[0]
        step = 256

        @pl.loop(0, tokens // step)
        def _(b):
            at = pl.ds(pl.multiple_of(b * step, step), step)
            turned = jnp.dot(s.left[at, :], s.basis[...], preferred_element_type=jnp.float32).T
            high = turned.astype(jnp.bfloat16)
            s.pair[:rank, at] = high
            s.pair[rank:, at] = (turned - high.astype(jnp.float32)).astype(jnp.bfloat16)

    def quarter(s, c):
        cols = pl.ds(pl.multiple_of(c * s.width, 128), s.width)
        both = jnp.dot(s.pair[...], s.right[:, cols], preferred_element_type=jnp.float32)
        value = both[:rank] + both[rank:]
        for g in range(n_f):
            for h in range(2):
                start = g * rows + h * half
                s.part[h, c, g] = value[start : start + half]

    first = (1, 2)
    second = (2, 1)

    def partials(i, s):
        token_product(i, s)
        loads[i, "right"].wait()
        quarter(s, flip(r, 3))
        if i == 0:
            pl.semaphore_wait(barrier, group - 1 + n_f - 1)
        s.fwd, s.keep = [], [None, None]
        for h in range(2):
            s.fwd.append(
                send(s.part.at[h, flip(r, 3)], s.fwd_in.at[h], {"rep": flip(r, first[h])})
            )
        for h in range(2):
            quarter(s, flip(r, first[h]))
            s.keep[h] = send(
                s.part.at[h, flip(r, first[h])], s.keep_in.at[h], {"rep": flip(r, first[h])}
            )
        quarter(s, r)

    def forward(s):
        s.last = []
        for h in range(2):
            s.fwd[h].wait_recv()
            c = flip(r, second[h])
            s.part[h, c] = s.part[h, c] + s.fwd_in[h]
            s.last.append(send(s.part.at[h, c], s.last_in.at[h], {"rep": c}))

    def scatter_rows(s):
        s.row = {}
        for h in range(2):
            s.keep[h].wait_recv()
            s.last[h].wait_recv()
            s.part[h, r] = s.part[h, r] + s.keep_in[h] + s.last_in[h]
            for k in range(1, n_f):
                g = lax.rem(f + k, n_f)
                s.row[k, h] = send(s.part.at[h, r, g], s.row_in.at[k - 1, h], {"fs": g})

    def squares(s):
        total = jnp.zeros((8, 128), jnp.float32)
        for h in range(2):
            value = s.part[h, r, f]
            for k in range(1, n_f):
                s.row[k, h].wait_recv()
                value = value + s.row_in[k - 1, h]
            s.part[h, r, f] = value
            square = value * value
            for a in range(half // 8):
                for b in range(s.width // 128):
                    total = total + square[a * 8 : a * 8 + 8, b * 128 : b * 128 + 128]
        s.near[place] = total
        s.near_copies = [
            send(s.near.at[place], s.near.at[place], neighbour(k)) for k in range(1, group)
        ]

    def squares_far(s):
        for copy in s.near_copies:
            copy.wait_recv()
        s.far[f] = jnp.sum(s.near[...], axis=0)
        s.far_copies = [
            send(s.far.at[f], s.far.at[f], {"fs": lax.rem(f + k, n_f)}) for k in range(1, n_f)
        ]

    def direction(i, s):
        loads[i, "mean"].wait()
        loads[i, "var"].wait()
        for copy in s.far_copies:
            copy.wait_recv()
        total = jnp.sum(jnp.sum(s.far[...], axis=0), keepdims=True)
        count = float(rank * s.width * REP * n_t)
        scale = 1.0 / jnp.maximum(jnp.sqrt(total / count), 1.0)
        for h in range(2):
            scaled = scale * s.part[h, r, f]
            at = slice(h * half, (h + 1) * half)
            new_mean = 0.8 * s.mean[at, :] + 0.2 * scaled
            new_var = 0.9 * s.var[at, :] + 0.1 * scaled * scaled
            rank_rows = pl.ds(pl.multiple_of(f * rows + h * half, 8), half)
            s.gathered[r, rank_rows, :] = new_mean / jnp.sqrt(new_var)
        own = s.gathered.at[r, pl.ds(pl.multiple_of(f * rows, 8), rows), :]
        s.ring = {k: send(own, own, {"fs": lax.rem(f + k, n_f)}) for k in range(1, n_f)}
        s.side = {}

    order = sorted(range(n_f), key=lambda k: min(k, n_f - k))

    def piece(s, c, k, h):
        g = lax.rem(f + n_f - k, n_f)
        return s.gathered.at[c, pl.ds(pl.multiple_of(g * rows + h * half, 8), half), :]

    def spread_one(s, k):
        if k > 0:
            s.ring[k].wait_recv()
        for h in range(2):
            own = piece(s, r, k, h)
            s.side[k, h] = send(own, own, {"rep": flip(r, second[h])})
        for h in range(2):
            own = piece(s, r, k, h)
            s.side[k, h, "own"] = send(own, own, {"rep": flip(r, first[h])})

    def spread_two(s, k):
        for h in range(2):
            s.side[k, h].wait_recv()
            passed = piece(s, flip(r, second[h]), k, h)
            s.side[k, h, "pass"] = send(passed, passed, {"rep": flip(r, first[h])})

    q, o = streams
    partials(0, q)
    forward(q)
    partials(1, o)
    scatter_rows(q)
    forward(o)
    squares(q)
    scatter_rows(o)
    squares_far(q)
    direction(0, q)
    squares(o)
    squares_far(o)
    spread_one(q, 0)
    direction(1, o)
    for j, k in enumerate(order):
        if j > 0:
            spread_one(q, k)
            spread_two(q, order[j - 1])
    spread_one(o, 0)
    spread_two(q, order[-1])
    for j, k in enumerate(order):
        if j > 0:
            spread_one(o, k)
            spread_two(o, order[j - 1])
    spread_two(o, order[-1])
    for s in streams:
        for k in range(n_f):
            for h in range(2):
                s.side[k, h, "own"].wait_recv()
                s.side[k, h, "pass"].wait_recv()
    for copy in pending:
        copy.wait_send()


def step_kernel(_, *refs):
    for i in range(2):
        basis, moved, weight = refs[3 * i : 3 * i + 3]
        step_ref, copy_ref = refs[6 + 2 * i : 8 + 2 * i]
        value = moved[0]
        high = value.astype(jnp.bfloat16)
        low = (value - high.astype(jnp.float32)).astype(jnp.bfloat16)
        step = jnp.dot(basis[...], high, preferred_element_type=jnp.float32) + jnp.dot(
            basis[...], low, preferred_element_type=jnp.float32
        )
        step_ref[...] = step
        copy_ref[...] = (weight[...] - 0.05 * step).astype(jnp.bfloat16)


def on_device(
    n_f, n_t,
    saved_latent, query_cotangent, mix_cotangent, head_outputs, query_weight, out_weight,
    query_basis, out_basis, query_mean, query_var, out_mean, out_var,
):
    f32, bf16 = jnp.float32, jnp.bfloat16
    rank = query_basis.shape[1]
    rows = rank // n_f
    half = rows // 2
    groups = (
        (saved_latent, query_cotangent, query_basis, query_mean, query_var),
        (mix_cotangent, head_outputs, out_basis, out_mean, out_var),
    )
    scratch, outs = [], []
    for left, right, basis, mean, _ in groups:
        w = right.shape[1] // REP
        scratch += [
            pltpu.VMEM(left.shape, bf16),
            pltpu.VMEM(right.shape, bf16),
            pltpu.VMEM(basis.shape, bf16),
            pltpu.VMEM((rows, w), f32),
            pltpu.VMEM((rows, w), f32),
            pltpu.VMEM((2 * rank, left.shape[0]), bf16),
            pltpu.VMEM((2, REP, n_f, half, w), f32),
            pltpu.VMEM((2, n_f, half, w), f32),
            pltpu.VMEM((2, n_f, half, w), f32),
            pltpu.VMEM((2, n_f, half, w), f32),
            pltpu.VMEM((n_f - 1, 2, half, w), f32),
            pltpu.VMEM((REP * n_t, 8, 128), f32),
            pltpu.VMEM((n_f, 8, 128), f32),
        ]
        outs.append(jax.ShapeDtypeStruct((REP, rank, w), f32))
    n_sem = 2 * (6 + 2 * (n_f - 1) + REP * n_t - 1 + (n_f - 1) + (n_f - 1) + 6 * n_f)
    moved_query, moved_out = pl.pallas_call(
        functools.partial(exchange_kernel, n_f, n_t, n_sem),
        out_shape=outs,
        in_specs=[pl.BlockSpec(memory_space=pl.ANY)] * 10,
        out_specs=[pl.BlockSpec(memory_space=pltpu.VMEM)] * 2,
        scratch_shapes=scratch
        + [
            pltpu.SemaphoreType.DMA((10,)),
            pltpu.SemaphoreType.DMA((n_sem,)),
            pltpu.SemaphoreType.DMA((n_sem,)),
        ],
        compiler_params=pltpu.CompilerParams(
            collective_id=0, has_side_effects=True, vmem_limit_bytes=48 * 1024 * 1024
        ),
        name="exchange",
    )(*groups[0], *groups[1])

    cuts = 2
    specs_in, specs_out, shapes = [], [], []
    for weight, basis, moved in (
        (query_weight, query_basis, moved_query),
        (out_weight, out_basis, moved_out),
    ):
        w = moved.shape[2]
        high = weight.shape[0] // cuts
        block = pl.BlockSpec((high, w), lambda c, b, at: (b, c))
        specs_in += [
            pl.BlockSpec((high, rank), lambda c, b, at: (at[0] * cuts + b, 0)),
            pl.BlockSpec((1, rank, w), lambda c, b, at: (c, 0, 0)),
            block,
        ]
        specs_out += [block, block]
        shapes += [
            jax.ShapeDtypeStruct(weight.shape, f32),
            jax.ShapeDtypeStruct(weight.shape, bf16),
        ]
    position = lax.axis_index("fs").astype(jnp.int32).reshape(1)
    query_step, query_copy, out_step, out_copy = pl.pallas_call(
        step_kernel,
        out_shape=shapes,
        grid_spec=pltpu.PrefetchScalarGridSpec(
            num_scalar_prefetch=1, grid=(REP, cuts), in_specs=specs_in, out_specs=specs_out
        ),
        compiler_params=pltpu.CompilerParams(
            dimension_semantics=("arbitrary", "arbitrary"), vmem_limit_bytes=32 * 1024 * 1024
        ),
        name="steps",
    )(position, query_basis, moved_query, query_weight, out_basis, moved_out, out_weight)
    return query_step, out_step, query_copy, out_copy


def solution(mesh):
    sizes = dict(mesh.shape)
    assert sizes["rep"] == REP
    placed = (
        P(("fs", "rep"), None),
        P(("fs", "rep"), "tp"),
        P(("fs", "rep"), None),
        P(("fs", "rep"), "tp"),
        P("fs", "tp"),
        P("fs", "tp"),
        P(),
        P(),
        P("fs", "tp"),
        P("fs", "tp"),
        P("fs", "tp"),
        P("fs", "tp"),
    )
    return jax.shard_map(
        functools.partial(on_device, sizes["fs"], sizes["tp"]),
        mesh=mesh,
        in_specs=placed,
        out_specs=(P("fs", "tp"), P("fs", "tp"), P("fs", "tp"), P("fs", "tp")),
        check_vma=False,
    )
```

time: 253 us -> 85.7 us (0.34); the launches traced: 249 us -> 85.4 us
  waiting for transfers between devices: 150 us -> 0 us
  Pallas kernels: 0 us -> 79.6 us
  matrix products: 55.5 us -> 0 us
  blocking collectives: 16.9 us -> 0 us
  between operations: 15.8 us -> 0.69 us
  other arithmetic: 6.95 us -> 0 us
    pallas_call x0 -> x2, Pallas kernels: none -> 79.6 us  [the longest x1 73.3 us: on_device(): pl.pallas_call(functools.partial(exchange_kernel, n_f, n_t, n_sem), out_s...]
    dot_general x6 -> x0, matrix products: 55.5 us -> none  [the longest x2 24.9 us: project(): lax.dot_general(basis.astype(jnp.float32), grad, (((0,), (0,)), ((), ()))...]
    all_gather x2 -> x0, waiting for transfers between devices: 53.5 us -> none  [the longest x1 30.8 us: on_device(): lax.all_gather(query_dir, 'fs', axis=0, tiled=True)]
    psum x1 -> x0, waiting for transfers between devices: 48.7 us -> none  [on_device(): query_proj, out_proj = lax.psum((query_shard, out_shard), 'rep')]
    reduce_scatter x2 -> x0, waiting for transfers between devices: 47.5 us -> none  [the longest x1 36.9 us: on_device(): lax.psum_scatter(query_early, 'fs', scatter_dimension=0, tiled=True)]
    psum x1 -> x0, blocking collectives: 16.9 us -> none  [on_device(): lax.psum((jnp.sum(query_proj * query_proj), jnp.sum(out_proj * out_proj))...]
    div x2 -> x0, other arithmetic: 3.63 us -> none  [moment_direction(): return new_mean / jnp.sqrt(new_var)]
    reduce_sum x2 -> x0, other arithmetic: 3.32 us -> none  [the longest x1 1.7 us: on_device(): jnp.sum(query_proj * query_proj)]
  transfers between devices with their start and end apart: 5 -> 0, of which waited for: 5 -> 0; matrix products, arithmetic and copies ran while one was open for 12% -> 0% of each run, Pallas kernels for 0% -> 0%
where the time goes in v1:
time: 85.7 us; the launch traced here: 85.4 us
  Pallas kernels  79.6 us (93%)
  local copies, waits for them, and re-layouts  5.12 us (6%)
    pallas_call x1, Pallas kernels, on_device(): pl.pallas_call(functools.partial(exchange_kernel, n_f, n_t, n_sem), out_s...  73.3 us
    pallas_call x1, Pallas kernels, on_device(): pl.pallas_call(step_kernel, out_shape=shapes, grid_spec=pltpu.PrefetchSca...  6.29 us
    unnamed x16, local copies, waits for them, and re-layouts  5.12 us

profile of v1, /device:TPU:0, one launch (start us, length us, event | category | flops | bytes accessed | tf_op | source)
XLA Modules:
  0.0 85.4 jit_solution(3736797250999147766)
XLA Ops:
  0.6 0.0 copy-start.1
  0.6 1.2 %copy-done.1 = bf16[2048,256]{1,0:T(8,128)(2,1)S(1)} copy-done((bf16[2048,256]{1,0:T(8,128)(2,1)S(1)}, bf16[2048,256]{1,0:T(8,128)(2,1)}, u32[]{:S(2)}) %copy-start.1) | copy-done | bytes 1048600
  1.9 0.0 copy-start.4
  1.9 1.0 %copy-done.4 = f32[64,1536]{1,0:T(8,128)S(1)} copy-done((f32[64,1536]{1,0:T(8,128)S(1)}, f32[64,1536]{1,0:T(8,128)}, u32[]{:S(2)}) %copy-start.4) | copy-done | bytes 393240
  2.9 0.0 copy-start.5
  2.9 1.0 %copy-done.5 = f32[64,1536]{1,0:T(8,128)S(1)} copy-done((f32[64,1536]{1,0:T(8,128)S(1)}, f32[64,1536]{1,0:T(8,128)}, u32[]{:S(2)}) %copy-start.5) | copy-done | bytes 393240
  3.9 0.0 copy-start.6
  3.9 0.9 %copy-done.6 = f32[64,1024]{1,0:T(8,128)S(1)} copy-done((f32[64,1024]{1,0:T(8,128)S(1)}, f32[64,1024]{1,0:T(8,128)}, u32[]{:S(2)}) %copy-start.6) | copy-done | bytes 262168
  4.8 0.0 copy-start.7
  4.8 0.9 %copy-done.7 = f32[64,1024]{1,0:T(8,128)S(1)} copy-done((f32[64,1024]{1,0:T(8,128)S(1)}, f32[64,1024]{1,0:T(8,128)}, u32[]{:S(2)}) %copy-start.7) | copy-done | bytes 262168
  5.8 0.0 copy-start
  5.8 0.0 copy-start.2
  5.8 0.0 copy-start.3
  5.8 73.3 %exchange.1 = (f32[4,256,384]{2,1,0:T(8,128)S(1)}, f32[4,256,256]{2,1,0:T(8,128)S(1)}) custom-call(bf16[768,2048]{1,0:T(8,128)(2,1)} %refs_0_.2, bf16[768,1536]{1,0:T(8,128)(2,1)} %refs_1_.1, bf16[2048,256]{1,0:T(8,128)(2,1)S(1)} %copy-done.1, f32[64,1536]{1,0:T(8,128)S(1)} %copy-done.4, f32[64,1536]{1,0:T(8,128)S(1)} %copy-done.5, ...), custom_call_target="tpu_custom_call" | custom-call | tf_op jit(solution)/shard_map/exchange/pallas_call | solution.py:300
  79.0 0.0 copy-done
  79.1 0.0 copy-done.2
  79.1 0.0 copy-done.3
  79.1 6.3 %steps.1 = (f32[512,1536]{1,0:T(8,128)}, bf16[512,1536]{1,0:T(8,128)(2,1)}, f32[1024,1024]{1,0:T(8,128)}, bf16[1024,1024]{1,0:T(8,128)(2,1)}) custom-call(s32[1]{0:T(128)} %bitcast._, bf16[2048,256]{1,0:T(8,128)(2,1)S(1)} %copy-done.1, f32[4,256,384]{2,1,0:T(8,128)S(1)} %get-tuple-element.10.refs_1_, f32[512,1536]{1,0:T(8,128)S(1)} %copy-done.3, ...), custom_call_target="tpu_custom_call" | custom-call | tf_op jit(solution)/shard_map/steps/pallas_call | solution.py:337
Async XLA Ops:
  0.6 1.2 %copy-start.1 = (bf16[2048,256]{1,0:T(8,128)(2,1)S(1)}, bf16[2048,256]{1,0:T(8,128)(2,1)}, u32[]{:S(2)}) copy-start(bf16[2048,256]{1,0:T(8,128)(2,1)} %refs_0_.3) | copy-start | bytes 3145732
  1.9 1.0 %copy-start.4 = (f32[64,1536]{1,0:T(8,128)S(1)}, f32[64,1536]{1,0:T(8,128)}, u32[]{:S(2)}) copy-start(f32[64,1536]{1,0:T(8,128)} %refs_3_.2) | copy-start | bytes 1179652
  2.9 1.0 %copy-start.5 = (f32[64,1536]{1,0:T(8,128)S(1)}, f32[64,1536]{1,0:T(8,128)}, u32[]{:S(2)}) copy-start(f32[64,1536]{1,0:T(8,128)} %refs_4_.1) | copy-start | bytes 1179652
  3.9 0.9 %copy-start.6 = (f32[64,1024]{1,0:T(8,128)S(1)}, f32[64,1024]{1,0:T(8,128)}, u32[]{:S(2)}) copy-start(f32[64,1024]{1,0:T(8,128)} %refs_8_.1) | copy-start | bytes 786436
  4.8 0.9 %copy-start.7 = (f32[64,1024]{1,0:T(8,128)S(1)}, f32[64,1024]{1,0:T(8,128)}, u32[]{:S(2)}) copy-start(f32[64,1024]{1,0:T(8,128)} %refs_9_.1) | copy-start | bytes 786436
  5.8 73.3 %copy-start = (bf16[4096,256]{1,0:T(8,128)(2,1)S(1)}, bf16[4096,256]{1,0:T(8,128)(2,1)}, u32[]{:S(2)}) copy-start(bf16[4096,256]{1,0:T(8,128)(2,1)} %refs_3_.3) | copy-start | bytes 6291460
  5.8 73.3 %copy-start.2 = (f32[1024,1024]{1,0:T(8,128)S(1)}, f32[1024,1024]{1,0:T(8,128)}, u32[]{:S(2)}) copy-start(f32[1024,1024]{1,0:T(8,128)} %refs_5_.3) | copy-start | bytes 12582916
  5.8 73.3 %copy-start.3 = (f32[512,1536]{1,0:T(8,128)S(1)}, f32[512,1536]{1,0:T(8,128)}, u32[]{:S(2)}) copy-start(f32[512,1536]{1,0:T(8,128)} %refs_2_.3) | copy-start | bytes 9437188

commit v2 on v1

--- a/solution.py
+++ b/solution.py
@@ -9,6 +9,8 @@
 
 MESH = pl.DeviceIdType.MESH
 REP = 4
+LANES = 128
+TOKEN_STEP = 256
 
 
 def flip(r, bits):
@@ -39,7 +41,8 @@
         s = Stream(STREAM_IN, ins[5 * i : 5 * i + 5])
         s.__dict__.update(zip(STREAM_SCRATCH, scratch[per * i : per * i + per]))
         s.gathered = outs[i]
-        s.width = s.part.shape[-1]
+        s.width = s.gathered.shape[-1]
+        s.pieces = s.width // LANES
         streams.append(s)
     load_sem, send_sem, recv_sem = scratch[2 * per :]
     f, r, t = lax.axis_index("fs"), lax.axis_index("rep"), lax.axis_index("tp")
@@ -64,11 +67,16 @@
     slot = 0
     for i, s in enumerate(streams):
         cols = pl.ds(pl.multiple_of(r * s.width, 128), s.width)
-        for name in ("basis", "left", "right", "mean", "var"):
-            src = getattr(s, name + "_hbm")
+        blocks = s.left.shape[0] // TOKEN_STEP
+        for name in ["basis", *range(blocks), "right", "mean", "var"]:
             if name in ("mean", "var"):
-                src = src.at[:, cols]
-            copy = pltpu.make_async_copy(src, getattr(s, name), load_sem.at[slot])
+                src, dst = getattr(s, name + "_hbm").at[:, cols], getattr(s, name)
+            elif name in ("basis", "right"):
+                src, dst = getattr(s, name + "_hbm"), getattr(s, name)
+            else:
+                at = pl.ds(name * TOKEN_STEP, TOKEN_STEP)
+                src, dst = s.left_hbm.at[at, :], s.left.at[at, :]
+            copy = pltpu.make_async_copy(src, dst, load_sem.at[slot])
             copy.start()
             loads[i, name] = copy
             slot += 1
@@ -88,80 +96,70 @@
             barrier, inc=1, device_id={"fs": lax.rem(f + k, n_f)}, device_id_type=MESH
         )
 
-    def token_product(i, s):
-        loads[i, "basis"].wait()
-        loads[i, "left"].wait()
-        tokens = s.left.shape[0]
-        step = 256
-
-        @pl.loop(0, tokens // step)
-        def _(b):
-            at = pl.ds(pl.multiple_of(b * step, step), step)
-            turned = jnp.dot(s.left[at, :], s.basis[...], preferred_element_type=jnp.float32).T
-            high = turned.astype(jnp.bfloat16)
-            s.pair[:rank, at] = high
-            s.pair[rank:, at] = (turned - high.astype(jnp.float32)).astype(jnp.bfloat16)
+    def token_product(i, s, b):
+        if b == 0:
+            loads[i, "basis"].wait()
+        loads[i, b].wait()
+        at = slice(b * TOKEN_STEP, (b + 1) * TOKEN_STEP)
+        turned = jnp.dot(s.left[at, :], s.basis[...], preferred_element_type=jnp.float32).T
+        high = turned.astype(jnp.bfloat16)
+        s.pair[:rank, at] = high
+        s.pair[rank:, at] = (turned - high.astype(jnp.float32)).astype(jnp.bfloat16)
 
     def quarter(s, c):
-        cols = pl.ds(pl.multiple_of(c * s.width, 128), s.width)
+        cols = pl.ds(pl.multiple_of(c * s.width, LANES), s.width)
         both = jnp.dot(s.pair[...], s.right[:, cols], preferred_element_type=jnp.float32)
         value = both[:rank] + both[rank:]
         for g in range(n_f):
             for h in range(2):
                 start = g * rows + h * half
-                s.part[h, c, g] = value[start : start + half]
+                for p in range(s.pieces):
+                    s.part[h, c, p, g] = value[start : start + half, p * LANES : (p + 1) * LANES]
 
     first = (1, 2)
     second = (2, 1)
 
-    def partials(i, s):
-        token_product(i, s)
-        loads[i, "right"].wait()
-        quarter(s, flip(r, 3))
-        if i == 0:
-            pl.semaphore_wait(barrier, group - 1 + n_f - 1)
-        s.fwd, s.keep = [], [None, None]
-        for h in range(2):
-            s.fwd.append(
-                send(s.part.at[h, flip(r, 3)], s.fwd_in.at[h], {"rep": flip(r, first[h])})
+    def send_fwd(s, p):
+        for h in range(2):
+            s.fwd[h, p] = send(
+                s.part.at[h, flip(r, 3), p], s.fwd_in.at[h, p], {"rep": flip(r, first[h])}
             )
-        for h in range(2):
-            quarter(s, flip(r, first[h]))
-            s.keep[h] = send(
-                s.part.at[h, flip(r, first[h])], s.keep_in.at[h], {"rep": flip(r, first[h])}
-            )
-        quarter(s, r)
-
-    def forward(s):
-        s.last = []
-        for h in range(2):
-            s.fwd[h].wait_recv()
+
+    def send_keep(s, p):
+        for h in range(2):
+            c = flip(r, first[h])
+            s.keep[h, p] = send(s.part.at[h, c, p], s.keep_in.at[h, p], {"rep": c})
+
+    def forward(s, p):
+        for h in range(2):
+            s.fwd[h, p].wait_recv()
             c = flip(r, second[h])
-            s.part[h, c] = s.part[h, c] + s.fwd_in[h]
-            s.last.append(send(s.part.at[h, c], s.last_in.at[h], {"rep": c}))
-
-    def scatter_rows(s):
-        s.row = {}
-        for h in range(2):
-            s.keep[h].wait_recv()
-            s.last[h].wait_recv()
-            s.part[h, r] = s.part[h, r] + s.keep_in[h] + s.last_in[h]
+            s.part[h, c, p] = s.part[h, c, p] + s.fwd_in[h, p]
+            s.last[h, p] = send(s.part.at[h, c, p], s.last_in.at[h, p], {"rep": c})
+
+    def scatter_rows(s, p):
+        for h in range(2):
+            s.keep[h, p].wait_recv()
+            s.last[h, p].wait_recv()
+            s.part[h, r, p] = s.part[h, r, p] + s.keep_in[h, p] + s.last_in[h, p]
             for k in range(1, n_f):
                 g = lax.rem(f + k, n_f)
-                s.row[k, h] = send(s.part.at[h, r, g], s.row_in.at[k - 1, h], {"fs": g})
+                s.row[k, h, p] = send(
+                    s.part.at[h, r, p, g], s.row_in.at[k - 1, h, p], {"fs": g}
+                )
 
     def squares(s):
         total = jnp.zeros((8, 128), jnp.float32)
-        for h in range(2):
-            value = s.part[h, r, f]
-            for k in range(1, n_f):
-                s.row[k, h].wait_recv()
-                value = value + s.row_in[k - 1, h]
-            s.part[h, r, f] = value
-            square = value * value
-            for a in range(half // 8):
-                for b in range(s.width // 128):
-                    total = total + square[a * 8 : a * 8 + 8, b * 128 : b * 128 + 128]
+        for p in range(s.pieces):
+            for h in range(2):
+                value = s.part[h, r, p, f]
+                for k in range(1, n_f):
+                    s.row[k, h, p].wait_recv()
+                    value = value + s.row_in[k - 1, h, p]
+                s.part[h, r, p, f] = value
+                square = value * value
+                for a in range(half // 8):
+                    total = total + square[a * 8 : a * 8 + 8]
         s.near[place] = total
         s.near_copies = [
             send(s.near.at[place], s.near.at[place], neighbour(k)) for k in range(1, group)
@@ -184,12 +182,14 @@
         count = float(rank * s.width * REP * n_t)
         scale = 1.0 / jnp.maximum(jnp.sqrt(total / count), 1.0)
         for h in range(2):
-            scaled = scale * s.part[h, r, f]
             at = slice(h * half, (h + 1) * half)
-            new_mean = 0.8 * s.mean[at, :] + 0.2 * scaled
-            new_var = 0.9 * s.var[at, :] + 0.1 * scaled * scaled
             rank_rows = pl.ds(pl.multiple_of(f * rows + h * half, 8), half)
-            s.gathered[r, rank_rows, :] = new_mean / jnp.sqrt(new_var)
+            for p in range(s.pieces):
+                cols = slice(p * LANES, (p + 1) * LANES)
+                scaled = scale * s.part[h, r, p, f]
+                new_mean = 0.8 * s.mean[at, cols] + 0.2 * scaled
+                new_var = 0.9 * s.var[at, cols] + 0.1 * scaled * scaled
+                s.gathered[r, rank_rows, cols] = new_mean / jnp.sqrt(new_var)
         own = s.gathered.at[r, pl.ds(pl.multiple_of(f * rows, 8), rows), :]
         s.ring = {k: send(own, own, {"fs": lax.rem(f + k, n_f)}) for k in range(1, n_f)}
         s.side = {}
@@ -217,18 +217,53 @@
             s.side[k, h, "pass"] = send(passed, passed, {"rep": flip(r, first[h])})
 
     q, o = streams
-    partials(0, q)
-    forward(q)
-    partials(1, o)
-    scatter_rows(q)
-    forward(o)
+    for s in streams:
+        s.fwd, s.keep, s.last, s.row = {}, {}, {}, {}
+    blocks = q.left.shape[0] // TOKEN_STEP
+    for b in range(blocks):
+        token_product(0, q, b)
+    loads[0, "right"].wait()
+    quarter(q, flip(r, 3))
+    pl.semaphore_wait(barrier, group - 1 + n_f - 1)
+    send_fwd(q, 0)
+    quarter(q, flip(r, 1))
+    quarter(q, flip(r, 2))
+    send_keep(q, 0)
+    for p in range(1, q.pieces - 1):
+        send_fwd(q, p)
+        send_keep(q, p)
+    quarter(q, r)
+    token_product(1, o, 0)
+    forward(q, 0)
+    send_fwd(q, q.pieces - 1)
+    send_keep(q, q.pieces - 1)
+    for b in range(1, blocks):
+        token_product(1, o, b)
+    for p in range(1, q.pieces - 1):
+        forward(q, p)
+    loads[1, "right"].wait()
+    quarter(o, flip(r, 3))
+    quarter(o, flip(r, 1))
+    quarter(o, flip(r, 2))
+    scatter_rows(q, 0)
+    forward(q, q.pieces - 1)
+    for p in range(o.pieces):
+        send_fwd(o, p)
+        send_keep(o, p)
+    quarter(o, r)
+    for p in range(1, q.pieces):
+        scatter_rows(q, p)
+    for p in range(o.pieces):
+        forward(o, p)
     squares(q)
-    scatter_rows(o)
+    scatter_rows(o, 0)
     squares_far(q)
+    for p in range(1, o.pieces):
+        scatter_rows(o, p)
     direction(0, q)
+    spread_one(q, 0)
     squares(o)
     squares_far(o)
-    spread_one(q, 0)
     direction(1, o)
     for j, k in enumerate(order):
         if j > 0:
@@ -287,24 +322,26 @@
             pltpu.VMEM((rows, w), f32),
             pltpu.VMEM((rows, w), f32),
             pltpu.VMEM((2 * rank, left.shape[0]), bf16),
-            pltpu.VMEM((2, REP, n_f, half, w), f32),
-            pltpu.VMEM((2, n_f, half, w), f32),
-            pltpu.VMEM((2, n_f, half, w), f32),
-            pltpu.VMEM((2, n_f, half, w), f32),
-            pltpu.VMEM((n_f - 1, 2, half, w), f32),
+            pltpu.VMEM((2, REP, w // LANES, n_f, half, LANES), f32),
+            pltpu.VMEM((2, w // LANES, n_f, half, LANES), f32),
+            pltpu.VMEM((2, w // LANES, n_f, half, LANES), f32),
+            pltpu.VMEM((2, w // LANES, n_f, half, LANES), f32),
+            pltpu.VMEM((n_f - 1, 2, w // LANES, half, LANES), f32),
             pltpu.VMEM((REP * n_t, 8, 128), f32),
             pltpu.VMEM((n_f, 8, 128), f32),
         ]
         outs.append(jax.ShapeDtypeStruct((REP, rank, w), f32))
-    n_sem = 2 * (6 + 2 * (n_f - 1) + REP * n_t - 1 + (n_f - 1) + (n_f - 1) + 6 * n_f)
+    pieces = sum(right.shape[1] // REP // LANES for _, right, *_ in groups)
+    n_sem = pieces * (6 + 2 * (n_f - 1)) + 2 * (REP * n_t - 1 + 2 * (n_f - 1) + 6 * n_f)
+    n_load = sum(4 + left.shape[0] // TOKEN_STEP for left, *_ in groups)
     moved_query, moved_out = pl.pallas_call(
         functools.partial(exchange_kernel, n_f, n_t, n_sem),
         out_shape=outs,
-        in_specs=[pl.BlockSpec(memory_space=pl.ANY)] * 10,
+        in_specs=[pl.BlockSpec(memory_space=pltpu.HBM)] * 10,
         out_specs=[pl.BlockSpec(memory_space=pltpu.VMEM)] * 2,
         scratch_shapes=scratch
         + [
-            pltpu.SemaphoreType.DMA((10,)),
+            pltpu.SemaphoreType.DMA((n_load,)),
             pltpu.SemaphoreType.DMA((n_sem,)),
             pltpu.SemaphoreType.DMA((n_sem,)),
         ],
@@ -312,7 +349,7 @@
             collective_id=0, has_side_effects=True, vmem_limit_bytes=48 * 1024 * 1024
         ),
         name="exchange",
-    )(*groups[0], *groups[1])
+    )(*(pltpu.with_memory_space_constraint(x, pltpu.HBM) for group in groups for x in group))
 
     cuts = 2
     specs_in, specs_out, shapes = [], [], []

time: 85.7 us -> 79.3 us (0.925)
  local copies, waits for them, and re-layouts: 5.12 us -> 0.02 us
  Pallas kernels: 79.6 us -> 78.4 us
    unnamed x16 -> x8, local copies, waits for them, and re-layouts: 5.12 us -> 0.02 us
    pallas_call x1, Pallas kernels: 73.3 us -> 72.1 us  [on_device(): pl.pallas_call(functools.partial(exchange_kernel, n_f, n_t, n_sem), out_s...]
where the time goes in v2:
time: 79.3 us; the launch traced here: 79.1 us
  Pallas kernels  78.4 us (99%)
    pallas_call x1, Pallas kernels, on_device(): pl.pallas_call(functools.partial(exchange_kernel, n_f, n_t, n_sem), out_s...  72.1 us
    pallas_call x1, Pallas kernels, on_device(): pl.pallas_call(step_kernel, out_shape=shapes, grid_spec=pltpu.PrefetchSca...  6.29 us

profile of v2, /device:TPU:0, one launch (start us, length us, event | category | flops | bytes accessed | tf_op | source)
XLA Modules:
  0.0 79.1 jit_solution(17500871784568539654)
XLA Ops:
  0.6 0.0 copy-start
  0.6 0.0 copy-start.1
  0.7 0.0 copy-start.2
  0.7 0.0 copy-start.3
  0.7 72.1 %exchange.1 = (f32[4,256,384]{2,1,0:T(8,128)S(1)}, f32[4,256,256]{2,1,0:T(8,128)S(1)}) custom-call(bf16[768,2048]{1,0:T(8,128)(2,1)} %refs_0_.2, bf16[768,1536]{1,0:T(8,128)(2,1)} %refs_1_.1, bf16[2048,256]{1,0:T(8,128)(2,1)} %refs_0_.3, f32[64,1536]{1,0:T(8,128)} %refs_3_.2, f32[64,1536]{1,0:T(8,128)} %refs_4_.1, bf16[768,4096]{1,0:T(8,128)(2,1)} %refs_5_.2, ...), custom_call_target="tpu_custom_call" | custom-call | tf_op jit(solution)/shard_map/exchange/pallas_call | solution.py:337
  72.8 0.0 copy-done
  72.8 0.0 copy-done.1
  72.8 0.0 copy-done.2
  72.8 0.0 copy-done.3
  72.8 6.3 %steps.1 = (f32[512,1536]{1,0:T(8,128)}, bf16[512,1536]{1,0:T(8,128)(2,1)}, f32[1024,1024]{1,0:T(8,128)}, bf16[1024,1024]{1,0:T(8,128)(2,1)}) custom-call(s32[1]{0:T(128)} %bitcast._, bf16[2048,256]{1,0:T(8,128)(2,1)S(1)} %copy-done.1, f32[4,256,384]{2,1,0:T(8,128)S(1)} %get-tuple-element.10.refs_1_, f32[512,1536]{1,0:T(8,128)S(1)} %copy-done.3, ...), custom_call_target="tpu_custom_call" | custom-call | tf_op jit(solution)/shard_map/steps/pallas_call | solution.py:374
Async XLA Ops:
  0.6 72.2 %copy-start = (bf16[4096,256]{1,0:T(8,128)(2,1)S(1)}, bf16[4096,256]{1,0:T(8,128)(2,1)}, u32[]{:S(2)}) copy-start(bf16[4096,256]{1,0:T(8,128)(2,1)} %refs_3_.3) | copy-start | bytes 6291460
  0.6 72.2 %copy-start.1 = (bf16[2048,256]{1,0:T(8,128)(2,1)S(1)}, bf16[2048,256]{1,0:T(8,128)(2,1)}, u32[]{:S(2)}) copy-start(bf16[2048,256]{1,0:T(8,128)(2,1)} %refs_0_.3) | copy-start | bytes 3145732
  0.7 72.2 %copy-start.2 = (f32[1024,1024]{1,0:T(8,128)S(1)}, f32[1024,1024]{1,0:T(8,128)}, u32[]{:S(2)}) copy-start(f32[1024,1024]{1,0:T(8,128)} %refs_5_.3) | copy-start | bytes 12582916
  0.7 72.2 %copy-start.3 = (f32[512,1536]{1,0:T(8,128)S(1)}, f32[512,1536]{1,0:T(8,128)}, u32[]{:S(2)}) copy-start(f32[512,1536]{1,0:T(8,128)} %refs_2_.3) | copy-start | bytes 9437188

commit v3 on v2

--- a/solution.py
+++ b/solution.py
@@ -26,7 +26,7 @@
         self.__dict__.update(zip(names, refs))
 
 
-STREAM_IN = ("left_hbm", "right_hbm", "basis_hbm", "mean_hbm", "var_hbm")
+STREAM_IN = ("left_hbm", "right_hbm", "basis_hbm", "mean_hbm", "var_hbm", "weight_hbm")
 STREAM_SCRATCH = (
     "left", "right", "basis", "mean", "var", "pair", "part", "fwd_in", "keep_in", "last_in",
     "row_in", "near", "far",
@@ -34,13 +34,13 @@
 
 
 def exchange_kernel(n_f, n_t, n_sem, *refs):
-    ins, outs, scratch = refs[:10], refs[10:12], refs[12:]
+    ins, outs, scratch = refs[:12], refs[12:16], refs[16:]
     streams = []
     per = len(STREAM_SCRATCH)
     for i in range(2):
-        s = Stream(STREAM_IN, ins[5 * i : 5 * i + 5])
+        s = Stream(STREAM_IN, ins[6 * i : 6 * i + 6])
         s.__dict__.update(zip(STREAM_SCRATCH, scratch[per * i : per * i + per]))
-        s.gathered = outs[i]
+        s.gathered, s.weight = outs[i], outs[2 + i]
         s.width = s.gathered.shape[-1]
         s.pieces = s.width // LANES
         streams.append(s)
@@ -64,22 +64,25 @@
         return copy
 
     loads = {}
-    slot = 0
-    for i, s in enumerate(streams):
+    slots = iter(range(load_sem.shape[0]))
+
+    def start_loads(i, s, names):
         cols = pl.ds(pl.multiple_of(r * s.width, 128), s.width)
-        blocks = s.left.shape[0] // TOKEN_STEP
-        for name in ["basis", *range(blocks), "right", "mean", "var"]:
+        for name in names:
             if name in ("mean", "var"):
                 src, dst = getattr(s, name + "_hbm").at[:, cols], getattr(s, name)
-            elif name in ("basis", "right"):
+            elif name in ("basis", "right", "weight"):
                 src, dst = getattr(s, name + "_hbm"), getattr(s, name)
             else:
                 at = pl.ds(name * TOKEN_STEP, TOKEN_STEP)
                 src, dst = s.left_hbm.at[at, :], s.left.at[at, :]
-            copy = pltpu.make_async_copy(src, dst, load_sem.at[slot])
+            copy = pltpu.make_async_copy(src, dst, load_sem.at[next(slots)])
             copy.start()
             loads[i, name] = copy
-            slot += 1
+
+    blocks = streams[0].left.shape[0] // TOKEN_STEP
+    main = ["basis", *range(blocks), "right"]
+    start_loads(0, streams[0], main)
 
     group = n_t * REP
     place = r * n_t + t
@@ -219,10 +222,10 @@
     q, o = streams
     for s in streams:
         s.fwd, s.keep, s.last, s.row = {}, {}, {}, {}
-    blocks = q.left.shape[0] // TOKEN_STEP
     for b in range(blocks):
         token_product(0, q, b)
     loads[0, "right"].wait()
+    start_loads(1, o, main)
     quarter(q, flip(r, 3))
     pl.semaphore_wait(barrier, group - 1 + n_f - 1)
     send_fwd(q, 0)
@@ -242,6 +245,8 @@
     for p in range(1, q.pieces - 1):
         forward(q, p)
     loads[1, "right"].wait()
+    for i, s in enumerate(streams):
+        start_loads(i, s, ["mean", "var", "weight"])
     quarter(o, flip(r, 3))
     quarter(o, flip(r, 1))
     quarter(o, flip(r, 2))
@@ -263,19 +268,23 @@
     direction(0, q)
     spread_one(q, 0)
     squares(o)
+    spread_one(q, order[1])
+    spread_two(q, order[0])
     squares_far(o)
+    spread_one(q, order[2])
+    spread_two(q, order[1])
     direction(1, o)
-    for j, k in enumerate(order):
-        if j > 0:
-            spread_one(q, k)
-            spread_two(q, order[j - 1])
+    for j in range(3, n_f):
+        spread_one(q, order[j])
+        spread_two(q, order[j - 1])
     spread_one(o, 0)
     spread_two(q, order[-1])
-    for j, k in enumerate(order):
-        if j > 0:
-            spread_one(o, k)
-            spread_two(o, order[j - 1])
+    for j in range(1, n_f):
+        spread_one(o, order[j])
+        spread_two(o, order[j - 1])
     spread_two(o, order[-1])
+    loads[0, "weight"].wait()
+    loads[1, "weight"].wait()
     for s in streams:
         for k in range(n_f):
             for h in range(2):
@@ -309,11 +318,11 @@
     rows = rank // n_f
     half = rows // 2
     groups = (
-        (saved_latent, query_cotangent, query_basis, query_mean, query_var),
-        (mix_cotangent, head_outputs, out_basis, out_mean, out_var),
+        (saved_latent, query_cotangent, query_basis, query_mean, query_var, query_weight),
+        (mix_cotangent, head_outputs, out_basis, out_mean, out_var, out_weight),
     )
     scratch, outs = [], []
-    for left, right, basis, mean, _ in groups:
+    for left, right, basis, *_ in groups:
         w = right.shape[1] // REP
         scratch += [
             pltpu.VMEM(left.shape, bf16),
@@ -333,12 +342,13 @@
         outs.append(jax.ShapeDtypeStruct((REP, rank, w), f32))
     pieces = sum(right.shape[1] // REP // LANES for _, right, *_ in groups)
     n_sem = pieces * (6 + 2 * (n_f - 1)) + 2 * (REP * n_t - 1 + 2 * (n_f - 1) + 6 * n_f)
-    n_load = sum(4 + left.shape[0] // TOKEN_STEP for left, *_ in groups)
-    moved_query, moved_out = pl.pallas_call(
+    outs += [jax.ShapeDtypeStruct(w.shape, f32) for w in (query_weight, out_weight)]
+    n_load = sum(5 + left.shape[0] // TOKEN_STEP for left, *_ in groups)
+    moved_query, moved_out, near_query, near_out = pl.pallas_call(
         functools.partial(exchange_kernel, n_f, n_t, n_sem),
         out_shape=outs,
-        in_specs=[pl.BlockSpec(memory_space=pltpu.HBM)] * 10,
-        out_specs=[pl.BlockSpec(memory_space=pltpu.VMEM)] * 2,
+        in_specs=[pl.BlockSpec(memory_space=pltpu.HBM)] * 12,
+        out_specs=[pl.BlockSpec(memory_space=pltpu.VMEM)] * 4,
         scratch_shapes=scratch
         + [
             pltpu.SemaphoreType.DMA((n_load,)),
@@ -346,7 +356,7 @@
             pltpu.SemaphoreType.DMA((n_sem,)),
         ],
         compiler_params=pltpu.CompilerParams(
-            collective_id=0, has_side_effects=True, vmem_limit_bytes=48 * 1024 * 1024
+            collective_id=0, has_side_effects=True, vmem_limit_bytes=34 * 1024 * 1024
         ),
         name="exchange",
     )(*(pltpu.with_memory_space_constraint(x, pltpu.HBM) for group in groups for x in group))
@@ -378,10 +388,14 @@
             num_scalar_prefetch=1, grid=(REP, cuts), in_specs=specs_in, out_specs=specs_out
         ),
         compiler_params=pltpu.CompilerParams(
-            dimension_semantics=("arbitrary", "arbitrary"), vmem_limit_bytes=32 * 1024 * 1024
+            dimension_semantics=("arbitrary", "arbitrary"), vmem_limit_bytes=20 * 1024 * 1024
         ),
         name="steps",
-    )(position, query_basis, moved_query, query_weight, out_basis, moved_out, out_weight)
+    )(
+        position,
+        pltpu.with_memory_space_constraint(query_basis, pltpu.HBM), moved_query, near_query,
+        pltpu.with_memory_space_constraint(out_basis, pltpu.HBM), moved_out, near_out,
+    )
     return query_step, out_step, query_copy, out_copy
 
 

time: 79.3 us -> 75.8 us (0.956)
  Pallas kernels: 78.4 us -> 74.8 us
    pallas_call x1, Pallas kernels: 72.1 us -> 66.2 us  [on_device(): pl.pallas_call(functools.partial(exchange_kernel, n_f, n_t, n_sem), out_s...]
    pallas_call x1, Pallas kernels: 6.29 us -> 8.6 us  [on_device(): pl.pallas_call(step_kernel, out_shape=shapes, grid_spec=pltpu.PrefetchSca...]
where the time goes in v3:
time: 75.8 us; the launch traced here: 75.5 us
  Pallas kernels  74.8 us (99%)
    pallas_call x1, Pallas kernels, on_device(): pl.pallas_call(functools.partial(exchange_kernel, n_f, n_t, n_sem), out_s...  66.2 us
    pallas_call x1, Pallas kernels, on_device(): pl.pallas_call(step_kernel, out_shape=shapes, grid_spec=pltpu.PrefetchSca...  8.6 us

profile of v3, /device:TPU:0, one launch (start us, length us, event | category | flops | bytes accessed | tf_op | source)
XLA Modules:
  0.0 75.5 jit_solution(9085616733140177622)
XLA Ops:
  0.6 66.2 %exchange.1 = (f32[4,256,384]{2,1,0:T(8,128)S(1)}, f32[4,256,256]{2,1,0:T(8,128)S(1)}, f32[512,1536]{1,0:T(8,128)S(1)}, f32[1024,1024]{1,0:T(8,128)S(1)}) custom-call(bf16[768,2048]{1,0:T(8,128)(2,1)} %refs_0_.2, bf16[768,1536]{1,0:T(8,128)(2,1)} %refs_1_.1, bf16[2048,256]{1,0:T(8,128)(2,1)} %refs_0_.3, f32[64,1536]{1,0:T(8,128)} %refs_3_.2, ...), custom_call_target="tpu_custom_call" | custom-call | tf_op jit(solution)/shard_map/exchange/pallas_call | solution.py:347
  66.9 8.6 %steps.1 = (f32[512,1536]{1,0:T(8,128)}, bf16[512,1536]{1,0:T(8,128)(2,1)}, f32[1024,1024]{1,0:T(8,128)}, bf16[1024,1024]{1,0:T(8,128)(2,1)}) custom-call(s32[1]{0:T(128)} %bitcast._, bf16[2048,256]{1,0:T(8,128)(2,1)} %refs_0_.3, f32[4,256,384]{2,1,0:T(8,128)S(1)} %get-tuple-element.12.refs_1_, f32[512,1536]{1,0:T(8,128)S(1)} %get-tuple-element.13.refs_2_, ...), custom_call_target="tpu_custom_call" | custom-call | tf_op jit(solution)/shard_map/steps/pallas_call | solution.py:384
